TPU v7x, 32 devices: a whole 2x2x4 slice. The times are simulated.
32 devices in a mesh: sp: 8 (over z, y), tp: 4 (over x, core).
Axes of the slice: x: 2, y: 2, z: 4, core: 2. Of those that a mesh axis runs over, the one named last changes fastest.
Arguments:
- resid: bfloat16 [12288, 2048], P(('sp', 'tp')), may hold values from -6 to 6
- cond: bfloat16 [2048], P('sp'), may hold values from -6 to 6
- mod_shift: bfloat16 [2048, 2048], P('sp', 'tp'), may hold values from -0.125 to 0.125
- mod_scale: bfloat16 [2048, 2048], P('sp', 'tp'), may hold values from -0.125 to 0.125
- mod_gate: bfloat16 [2048, 2048], P('sp', 'tp'), may hold values from -0.125 to 0.125
- norm_gain: float32 [2048], replicated, may hold values from 0.1 to 1.9
- context: bfloat16 [512, 2048], P('sp'), may hold values from -6 to 6
- w_query: bfloat16 [2048, 2048], P(None, 'tp'), may hold values from -0.125 to 0.125
- w_key: bfloat16 [2048, 2048], P(None, 'tp'), may hold values from -0.125 to 0.125
- w_value: bfloat16 [2048, 2048], P(None, 'tp'), may hold values from -0.125 to 0.125
- query_gain: float32 [128], replicated, may hold values from 0.5 to 6, as said below
- key_gain: float32 [128], replicated, may hold values from 0.5 to 6, as said below
- offset_bias: float32 [16, 15, 31], P('tp'), may hold values from -4 to 4
- context_bias: float32 [16], P('tp'), may hold values from -4.5 to 1
- w_out: bfloat16 [2048, 2048], replicated, may hold values from -0.5 to 0.5
Outputs:
- mixed: bfloat16 [12288, 2048], P(('sp', 'tp'))
Inputs may be any that keep to these rules, and one draw needn't show every extreme that they name: `query_gain`: positive gains. `key_gain`: positive gains.
All inputs are finite; a program needn't handle non-finite values.
Results may differ from a plain program's by a relative error of at most 0.0085.
The roundings to bfloat16 on the way count: a program that leaves them out, or rounds other values in their place, can miss the bound.
Values may be sent and summed in bfloat16 or wider, within the bound.
A program may use at most 128 MiB of HBM per device.

v0:
```python
import jax
import jax.numpy as jnp
from jax import lax
from jax.sharding import PartitionSpec as P

HEAD_DIM = 128
GRID_W = 64
WIN_ROWS = 8
WIN_COLS = 16
R_DEV = 24


EPS = 1e-06


def padded_2(cells, sides, width):
    for axis, dim in sides:
        count = lax.axis_size(axis)
        ends = count - 1
        head = lax.slice_in_dim(cells, 0, width, axis=dim)
        tail = lax.slice_in_dim(cells, cells.shape[dim] - width, cells.shape[dim], axis=dim)
        cells = jnp.concatenate(
            [
                lax.ppermute(tail, axis, [(i, (i + 1) % count) for i in range(ends)]),
                cells,
                lax.ppermute(head, axis, [((i + 1) % count, i) for i in range(ends)]),
            ],
            axis=dim,
        )
    return cells


def head_norm(values, gain, heads_local):
    count = values.shape[0]
    split = values.reshape(count, heads_local, -1)
    scaled = split * lax.rsqrt(jnp.mean(split * split, axis=-1, keepdims=True) + EPS) * gain
    return scaled.reshape(count, -1).astype(jnp.bfloat16)


def project_context(rows_in, norm_gain, w_key, w_value, key_gain, heads_local):
    floats = rows_in.astype(jnp.float32)
    inverse = lax.rsqrt(jnp.mean(floats * floats, axis=-1, keepdims=True) + EPS)
    normed = (floats * inverse * norm_gain).astype(jnp.bfloat16)
    keys = head_norm(
        jnp.dot(normed, w_key, preferred_element_type=jnp.float32), key_gain, heads_local
    )
    values = jnp.dot(normed, w_value, preferred_element_type=jnp.float32).astype(jnp.bfloat16)
    return (keys, values)


def attend_rows(
    queries, key_at, value_at, row_offset, offset_bias, ctx_key, ctx_value, context_bias
):
    grid_w = queries.shape[1]
    columns = jnp.arange(grid_w, dtype=jnp.int32)
    col_begin = jnp.clip(columns - WIN_COLS // 2, 0, grid_w - WIN_COLS)
    valid = (columns[None, :] >= col_begin[:, None]) & (
        columns[None, :] < col_begin[:, None] + WIN_COLS
    )
    col_offset = jnp.clip(columns[None, :] - columns[:, None] + WIN_COLS - 1, 0, 2 * WIN_COLS - 2)
    col_onehot = (col_offset[..., None] == jnp.arange(2 * WIN_COLS - 1, dtype=jnp.int32)).astype(
        jnp.float32
    )
    row_onehot = (
        row_offset[:, :, None] == jnp.arange(2 * WIN_ROWS - 1, dtype=jnp.int32)[None, None, :]
    ).astype(jnp.float32)
    bias = jnp.einsum(
        "nir,hrj,ckj->nhcik", row_onehot, offset_bias, col_onehot, precision=lax.Precision.HIGHEST
    )
    factor = HEAD_DIM ** (-0.5)
    s_win = (
        jnp.stack(
            [
                jnp.einsum(
                    "nchd,nkhd->nhck", queries, key_at(i), preferred_element_type=jnp.float32
                )
                for i in range(WIN_ROWS)
            ],
            axis=3,
        )
        * factor
        + bias
    )
    s_win = jnp.where(valid[None, None, :, None, :], s_win, -1e30)
    s_ctx = (
        jnp.einsum("nchd,jhd->nhcj", queries, ctx_key, preferred_element_type=jnp.float32) * factor
    )
    s_ctx = s_ctx + context_bias[None, :, None, None]
    top = jnp.maximum(jnp.max(s_win, axis=(3, 4)), jnp.max(s_ctx, axis=3))
    e_win = jnp.exp(s_win - top[..., None, None])
    e_ctx = jnp.exp(s_ctx - top[..., None])
    total = jnp.sum(e_win, axis=(3, 4)) + jnp.sum(e_ctx, axis=3)
    p_win = (e_win / total[..., None, None]).astype(jnp.bfloat16)
    p_ctx = (e_ctx / total[..., None]).astype(jnp.bfloat16)
    out = jnp.einsum("nhcj,jhd->nchd", p_ctx, ctx_value, preferred_element_type=jnp.float32)
    for i in range(WIN_ROWS):
        out = out + jnp.einsum(
            "nhck,nkhd->nchd", p_win[:, :, :, i], value_at(i), preferred_element_type=jnp.float32
        )
    count = queries.shape[0]
    return out.astype(jnp.bfloat16).reshape(count * grid_w, -1)


def shards(
    resid,
    cond,
    mod_shift,
    mod_scale,
    mod_gate,
    norm_gain,
    context,
    w_query,
    w_key,
    w_value,
    query_gain,
    key_gain,
    offset_bias,
    context_bias,
    w_out,
):
    heads_local = offset_bias.shape[0]
    width = w_query.shape[1]
    lifted = jax.nn.silu(cond.astype(jnp.float32)).astype(jnp.bfloat16)
    shift_part = jnp.dot(lifted, mod_shift, preferred_element_type=jnp.float32)
    scale_part = jnp.dot(lifted, mod_scale, preferred_element_type=jnp.float32)
    gate_part = jnp.dot(lifted, mod_gate, preferred_element_type=jnp.float32)
    summed = lax.psum((shift_part, scale_part, gate_part), "sp")
    shift, scale, gate = (
        lax.all_gather(summed[0], "tp", axis=0, tiled=True),
        lax.all_gather(summed[1], "tp", axis=0, tiled=True),
        lax.all_gather(summed[2], "tp", axis=0, tiled=True),
    )
    floats = resid.astype(jnp.float32)
    inverse = lax.rsqrt(jnp.mean(floats * floats, axis=-1, keepdims=True) + EPS)
    normed = (floats * inverse * norm_gain * (1.0 + scale) + shift).astype(jnp.bfloat16)
    piece = lax.all_gather(normed, "tp", axis=0, tiled=True)
    queries = head_norm(
        jnp.dot(piece, w_query, preferred_element_type=jnp.float32), query_gain, heads_local
    )
    keys = head_norm(
        jnp.dot(piece, w_key, preferred_element_type=jnp.float32), key_gain, heads_local
    )
    values = jnp.dot(piece, w_value, preferred_element_type=jnp.float32).astype(jnp.bfloat16)
    projected = jnp.concatenate([queries, keys, values], axis=1)
    query = projected[:, :width]
    key_value = projected[:, width:]
    keys, values = project_context(
        lax.all_gather(context, "sp", axis=0, tiled=True),
        norm_gain,
        w_key,
        w_value,
        key_gain,
        heads_local,
    )
    ctx_both = jnp.concatenate([keys, values], axis=1)
    ctx_key = ctx_both[:, :width]
    ctx_value = ctx_both[:, width:]
    ctx_count = ctx_key.shape[0]
    ctx_key = ctx_key.reshape(ctx_count, heads_local, HEAD_DIM)
    ctx_value = ctx_value.reshape(ctx_count, heads_local, HEAD_DIM)
    reach = WIN_ROWS // 2
    grid = key_value.reshape(R_DEV, GRID_W, 2 * width)
    padded = padded_2(grid, (("sp", 0),), reach)
    padded = padded.reshape(R_DEV + 2 * reach, GRID_W, 2, heads_local, HEAD_DIM)
    total_rows = R_DEV * lax.axis_size("sp")
    first = lax.axis_index("sp") * R_DEV
    global_rows = first + jnp.arange(R_DEV, dtype=jnp.int32)
    row_start = jnp.clip(global_rows - reach, 0, total_rows - WIN_ROWS)
    window_rows = jnp.arange(WIN_ROWS, dtype=jnp.int32)[None, :]
    row_offset = row_start[:, None] + window_rows - global_rows[:, None] + WIN_ROWS - 1
    queries = query.reshape(R_DEV, GRID_W, heads_local, HEAD_DIM)
    upper = min(reach, R_DEV)
    lower = max(upper, R_DEV - reach)
    edge_rows = list(range(upper)) + list(range(lower, R_DEV))
    edge_index = jnp.array(edge_rows, dtype=jnp.int32)
    edge_window = (jnp.take(row_start, edge_index) - first + reach)[:, None] + window_rows
    edge_kv = jnp.take(padded, edge_window, axis=0)
    edge_out = attend_rows(
        jnp.take(queries, edge_index, axis=0),
        lambda i: edge_kv[:, i, :, 0],
        lambda i: edge_kv[:, i, :, 1],
        jnp.take(row_offset, edge_index, axis=0),
        offset_bias,
        ctx_key,
        ctx_value,
        context_bias,
    )
    pieces = [edge_out[: upper * GRID_W]]
    middle = lower - upper
    inner_out = attend_rows(
        queries[upper:lower],
        lambda i: padded[upper + i : upper + i + middle, :, 0],
        lambda i: padded[upper + i : upper + i + middle, :, 1],
        row_offset[upper:lower],
        offset_bias,
        ctx_key,
        ctx_value,
        context_bias,
    )
    pieces.append(inner_out)
    pieces.append(edge_out[upper * GRID_W :])
    attended = jnp.concatenate(pieces, axis=0)
    full_rows = lax.all_to_all(attended, "tp", split_axis=0, concat_axis=1, tiled=True)
    result = jnp.dot(full_rows, w_out, preferred_element_type=jnp.float32)
    return (floats + gate * result).astype(jnp.bfloat16)


def solution(mesh):
    in_specs = (
        P(("sp", "tp"), None),
        P("sp"),
        P("sp", "tp"),
        P("sp", "tp"),
        P("sp", "tp"),
        P(),
        P("sp", None),
        P(None, "tp"),
        P(None, "tp"),
        P(None, "tp"),
        P(),
        P(),
        P("tp", None, None),
        P("tp"),
        P(),
    )
    out_specs = P(("sp", "tp"), None)
    return jax.shard_map(shards, mesh=mesh, in_specs=in_specs, out_specs=out_specs, check_vma=False)
```

profile of v0, /device:TPU:0, one launch (start us, length us, event | category | flops | bytes accessed | tf_op | source)
XLA Modules:
  0.0 350.9 jit_solution(10941702433033910941)
XLA Ops:
  11.3 24.2 %all-reduce = (f32[512]{0:T(512)S(1)}, f32[512]{0:T(512)S(1)}, f32[512]{0:T(512)}) all-reduce(f32[512]{0:T(512)S(1)} %bitcast.429, f32[512]{0:T(512)S(1)} %bitcast.430, f32[512]{0:T(512)S(1)} %bitcast.431), channel_id=1, replica_groups=mesh['sp'=8,'tp'=4] {'sp'}, use_global_device_ids=true, to_apply=%region_5.6 | all-reduce | flops 1536 | bytes 12288 | tf_op jit(solution)/shard_map/psum | solution.py:127
  35.4 5.2 %all-gather.2 = f32[4,1,512]{2,1,0:T(1,128)S(1)} all-gather(f32[1,1,512]{2,1,0:T(1,128)S(1)} %bitcast.435), channel_id=1, replica_groups=mesh['sp'=8,'tp'=4] {'tp'}, dimensions={0}, use_global_device_ids=true | all-gather | bytes 10240 | tf_op jit(solution)/shard_map/all_gather | solution.py:129
  40.6 5.2 %all-gather.1 = f32[4,1,512]{2,1,0:T(1,128)S(1)} all-gather(f32[1,1,512]{2,1,0:T(1,128)S(1)} %bitcast.434), channel_id=1, replica_groups=mesh['sp'=8,'tp'=4] {'tp'}, dimensions={0}, use_global_device_ids=true | all-gather | bytes 10240 | tf_op jit(solution)/shard_map/all_gather | solution.py:130
  54.6 6.0 %fusion.25 = f32[64,64,4,8,8]{1,4,3,2,0:T(8,128)} fusion(f32[64,64,4,15]{1,3,2,0:T(8,128)S(1)} %fusion.64, s32[8,8]{1,0:T(8,128)S(1)} %gather_fusion.3), kind=kOutput, calls=%fused_computation.68 | convolution fusion | flops 188744640 | bytes 5177600 | tf_op jit(solution)/shard_map/nir,hrj,ckj->nhcik/dot_general | solution.py:67
  60.5 9.6 %copy.413 = f32[64,64,4,8,8]{0,1,2,3,4:T(8,128)} copy(f32[64,64,4,8,8]{1,4,3,2,0:T(8,128)} %fusion.25) | data formatting | bytes 8388608 | tf_op jit(solution)/shard_map/nir,hrj,ckj->nhcik/dot_general | solution.py:67
  70.4 12.2 %fusion.23 = f32[64,64,4,16,8]{1,3,4,2,0:T(8,128)} fusion(f32[64,64,4,15]{1,3,2,0:T(8,128)} %copy-done.7, s32[16,8]{0,1:T(8,128)S(1)} %copy.455), kind=kOutput, calls=%fused_computation.66 | convolution fusion | flops 377489280 | bytes 9372160 | tf_op jit(solution)/shard_map/nir,hrj,ckj->nhcik/dot_general | solution.py:67
  82.6 18.2 %copy.456 = f32[64,64,4,16,8]{0,1,2,3,4:T(8,128)} copy(f32[64,64,4,16,8]{1,3,4,2,0:T(8,128)} %fusion.23) | data formatting | bytes 16777216 | tf_op jit(solution)/shard_map/nir,hrj,ckj->nhcik/dot_general | solution.py:67
  109.5 6.7 %bitcast_reduce_fusion.2 = (f32[1536,4]{0,1:T(4,128)S(1)}, f32[1536,512]{0,1:T(8,128)S(1)}) fusion(bf16[1536,2048]{1,0:T(8,128)(2,1)} %all-gather.8.cloned.1.call-done, bf16[2048,512]{1,0:T(8,128)(2,1)S(1)} %copy-done), kind=kOutput, calls=%fused_computation.51 | convolution fusion | flops 3222792192 | bytes 11558912 | tf_op jit(solution)/shard_map/dot_general | solution.py:141
  125.4 4.7 %concatenate.18 = bf16[24,64,2,4,128]{4,3,2,1,0:T(4,128)(2,1)S(1)} reshape(bf16[1536,1024]{1,0:T(8,128)(2,1)} %copy.406) | data formatting | bytes 6291456 | tf_op jit(solution)/shard_map/concatenate | solution.py:22
  132.8 8.2 %fusion.117 = (bf16[16,64,1,4,128]{4,3,2,1,0:T(4,128)(2,1)}, bf16[16,64,1,4,128]{4,3,2,1,0:T(4,128)(2,1)}, bf16[16,64,1,4,128]{4,3,2,1,0:T(4,128)(2,1)}, bf16[16...) fusion(bf16[24,64,2,4,128]{4,3,2,1,0:T(4,128)(2,1)S(1)} %concat, ...), kind=kLoop, calls=%fused_computation.262 | loop fusion | bytes 33554432 | tf_op jit(solution)/shard_map/slice | solution.py:193
  140.9 3.7 %bitcast_reduce_fusion.3 = (f32[1536,4]{0,1:T(4,128)S(1)}, f32[1536,512]{0,1:T(8,128)S(1)}) fusion(bf16[1536,2048]{1,0:T(8,128)(2,1)S(1)} %bitcast.437, bf16[2048,512]{1,0:T(8,128)(2,1)S(1)} %copy-done.38), kind=kOutput, calls=%fused_computation.55 | convolution fusion | flops 3222792192 | bytes 11558912 | tf_op jit(solution)/shard_map/dot_general | solution.py:138
  159.1 6.5 %copy-done.6 = f32[16,4,64,8,64]{2,4,1,0,3:T(8,128)} copy-done((f32[16,4,64,8,64]{2,4,1,0,3:T(8,128)}, f32[16,4,64,8,64]{2,4,1,0,3:T(8,128)S(1)}, u32[]{:S(2)}) %copy-start.6) | copy-done | bytes 8388632
  167.8 4.5 %slice-done.5 = s8[4194304]{0:T(1024)(128)(4,1)S(1)} async-done(((s8[16777216]{0:T(1024)(128)(4,1)}), s8[4194304]{0:T(1024)(128)(4,1)S(1)}, s32[]{:S(2)}) %slice-start.5) | async-done | bytes 4194328
  172.3 13.0 %fusion.113 = (f32[16,4,64]{2,1,0:T(4,128)S(1)}, f32[16,4,64,8,64]{2,4,1,0,3:T(8,128)}) fusion(f32[64,64,4,16,8]{0,1,2,3,4:T(8,128)S(1)} %bitcast.409, f32[16,4,64,8,64]{2,4,1,0,3:T(8,128)} %copy-done.6, pred[64,64]{0,1:T(8,128)(4,1)S(1)} %fusion.101), kind=kLoop, calls=%fused_computation.260 | loop fusion | flops 8384512 | bytes 25186304 | tf_op jit(solution)/shard_map/reduce_max | solution.py:89
  198.7 5.4 %collective-permute-start = (bf16[4,64,1024]{2,1,0:T(8,128)(2,1)}, bf16[4,64,1024]{2,1,0:T(8,128)(2,1)}, u32[]{:S(2)}, u32[]{:S(2)}) collective-permute-start(bf16[4,64,1024]{2,1,0:T(8,128)(2,1)} %bitcast.24), channel_id=1, source_target_pairs={{0,4},{4,8},{8,12},{12,16},{16,20},{20,24},{24,28},{1,5},{5,9},{9,... | collective-permute-start | bytes 1572872 | tf_op jit(solution)/shard_map/ppermute | solution.py:24
  204.0 8.6 %fusion.1 = f32[16,4,64]{2,1,0:T(4,128)S(1)} fusion(f32[16,4,64,8,64]{2,4,1,0,3:T(8,128)} %get-tuple-element.9, f32[16,4,64]{2,1,0:T(4,128)S(1)} %copy.458), kind=kLoop, calls=%fused_computation.8 | loop fusion | flops 4190208 | bytes 8421376 | tf_op jit(solution)/shard_map/reduce_sum | solution.py:92
  212.6 7.7 %divide_convert_fusion = bf16[16,4,64,8,64]{2,4,1,0,3:T(8,128)(2,1)S(1)} fusion(f32[16,4,64,8,64]{2,4,1,0,3:T(8,128)} %get-tuple-element.9, f32[16,4,64]{2,1,0:T(4,128)S(1)} %copy.462, f32[16,4,64]{2,1,0:T(4,128)S(1)} %copy.458), kind=kLoop, calls=%fused_computation.6 | loop fusion | flops 6291456 | bytes 12615680 | tf_op jit(solution)/shard_map/convert_element_type | solution.py:93
  243.9 8.1 %gather_fusion.2 = bf16[64,64,2,4,128]{4,1,3,2,0:T(8,128)(2,1)} fusion(bf16[32,64,2,4,128]{4,1,3,2,0:T(8,128)(2,1)} %pad_maximum_fusion, s32[1024]{0:T(1024)S(1)} %pad_clamp_fusion), kind=kCustom, calls=%fused_computation.2 | custom fusion | bytes 16777472 | tf_op jit(solution)/shard_map/jit(_take)/gather | solution.py:177
  252.0 7.5 %copy_select_fusion = bf16[8,8,64,2,4,128]{5,2,4,0,3,1:T(8,128)(2,1)} fusion(bf16[8,8,64,2,4,128]{5,2,4,3,1,0:T(8,128)(2,1)} %bitcast.415, pred[8,8]{0,1:T(8,128)(4,1)S(1)} %fusion.107), kind=kLoop, calls=%fused_computation.14 | loop fusion | flops 4194304 | bytes 16777280 | tf_op jit(solution)/shard_map/jit(_take)/select_n | solution.py:177
  278.9 12.4 %fusion.115 = (f32[8,4,64]{2,1,0:T(4,128)S(1)}, f32[8,4,64,8,64]{2,4,1,0,3:T(8,128)}) fusion(f32[64,64,4,8,8]{0,1,2,3,4:T(8,128)} %copy.413, f32[8,4,64,8,64]{2,4,1,0,3:T(8,128)} %fusion.37, pred[64,64]{0,1:T(8,128)(4,1)S(1)} %fusion.101), kind=kLoop, calls=%fused_computation.261 | loop fusion | flops 4192256 | bytes 12595200 | tf_op jit(solution)/shard_map/reduce_max | solution.py:89
  292.6 4.9 %fusion.4 = f32[8,4,64]{2,1,0:T(4,128)S(1)} fusion(f32[8,4,64,8,64]{2,4,1,0,3:T(8,128)} %get-tuple-element.11, f32[8,4,64]{2,1,0:T(4,128)S(1)} %copy.415), kind=kLoop, calls=%fused_computation.19 | loop fusion | flops 2095104 | bytes 4210688 | tf_op jit(solution)/shard_map/reduce_sum | solution.py:92
  309.5 4.3 %all-to-all-start = ((bf16[4,384,512]{1,2,0:T(8,128)(2,1)}), bf16[4,384,512]{1,2,0:T(8,128)(2,1)}, u32[]{:S(2)}, u32[]{:S(2)}) async-start(bf16[4,384,512]{1,2,0:T(8,128)(2,1)} %copy.480), calls=%async_computation | async-start | bytes 3145728 | tf_op jit(solution)/shard_map/all_to_all | solution.py:203
  313.8 21.0 %all-gather = f32[4,1,512]{2,1,0:T(1,128)S(1)} all-gather(f32[1,1,512]{2,1,0:T(1,128)S(1)} %bitcast.433), channel_id=1, replica_groups=mesh['sp'=8,'tp'=4] {'tp'}, dimensions={0}, use_global_device_ids=true | all-gather | bytes 10240 | tf_op jit(solution)/shard_map/all_gather | solution.py:131
  334.8 9.1 %fusion.17 = bf16[384,2048]{1,0:T(8,128)(2,1)} fusion(bf16[384,2048]{1,0:T(8,128)(2,1)} %param.16, bf16[384,2048]{0,1:T(8,128)(2,1)} %bitcast.128, bf16[2048,2048]{1,0:T(8,128)(2,1)} %param.30, f32[2048]{0:T(1024)S(1)} %bitcast.432), kind=kOutput, calls=%fused_computation.47 | convolution fusion | flops 3224371200 | bytes 13115392 | tf_op jit(solution)/shard_map/dot_general | solution.py:204
  (232 shorter events, 119.5 us)
Async XLA Ops:
  6.5 96.5 %copy-start = (bf16[2048,512]{1,0:T(8,128)(2,1)S(1)}, bf16[2048,512]{1,0:T(8,128)(2,1)}, u32[]{:S(2)}) copy-start(bf16[2048,512]{1,0:T(8,128)(2,1)} %param.24) | copy-start | bytes 6291460
  6.5 44.3 %copy-start.34 = (s32[8]{0:T(128)S(1)}, s32[8]{0:T(128)}, u32[]{:S(2)}) copy-start(s32[8]{0:T(128)} %constant.131) | copy-start | bytes 100
  6.5 45.7 %copy-start.28 = (f32[4,15,31]{2,0,1:T(4,128)S(1)}, f32[4,15,31]{2,0,1:T(4,128)}, u32[]{:S(2)}) copy-start(f32[4,15,31]{2,0,1:T(4,128)} %param.28) | copy-start | bytes 22324
  6.5 94.4 %all-gather.6.cloned.1.call-start = ((), (), s32[]{:S(2)}) async-start(), calls=%async_computation.1 | async-start | bytes 2359296 | tf_op jit(solution)/shard_map/all_gather | solution.py:148
  7.3 102.3 %all-gather.8.cloned.1.call-start = ((), (), s32[]{:S(2)}) async-start(), calls=%async_computation.2 | async-start | bytes 7864320 | tf_op jit(solution)/shard_map/all_gather | solution.py:136
  82.6 18.3 %copy-start.32 = (f32[128]{0:T(128)S(1)}, f32[128]{0:T(128)}, u32[]{:S(2)}) copy-start(f32[128]{0:T(128)} %param.26) | copy-start | bytes 1540
  82.6 18.3 %copy-start.33 = (f32[128]{0:T(128)S(1)}, f32[128]{0:T(128)}, u32[]{:S(2)}) copy-start(f32[128]{0:T(128)} %param.27) | copy-start | bytes 1540
  82.6 20.4 %copy-start.29 = (f32[2048]{0:T(1024)S(1)}, f32[2048]{0:T(1024)}, u32[]{:S(2)}) copy-start(f32[2048]{0:T(1024)} %param.21) | copy-start | bytes 24580
  109.5 7.1 %copy-start.35 = (bf16[1536,2048]{1,0:T(8,128)(2,1)S(1)}, bf16[1536,2048]{1,0:T(8,128)(2,1)}, u32[]{:S(2)}) copy-start(bf16[1536,2048]{1,0:T(8,128)(2,1)} %all-gather.8.cloned.1.call-done) | copy-start | bytes 18874372
  130.1 10.8 %slice-start.8 = ((s8[6291456]{0:T(1024)(128)(4,1)}), s8[4194304]{0:T(1024)(128)(4,1)S(1)}, s32[]{:S(2)}) async-start(s8[6291456]{0:T(1024)(128)(4,1)} %bitcast.436), calls=%async_computation.11 | async-start | bytes 8388608
  132.7 8.2 %slice-start.9 = ((s8[6291456]{0:T(1024)(128)(4,1)}), s8[2097152]{0:T(1024)(128)(4,1)S(1)}, s32[]{:S(2)}) async-start(s8[6291456]{0:T(1024)(128)(4,1)} %bitcast.436), calls=%async_computation.12 | async-start | bytes 4194304
  132.7 8.2 %copy-start.38 = (bf16[2048,512]{1,0:T(8,128)(2,1)S(1)}, bf16[2048,512]{1,0:T(8,128)(2,1)}, u32[]{:S(2)}) copy-start(bf16[2048,512]{1,0:T(8,128)(2,1)} %param.23) | copy-start | bytes 6291460
  157.0 10.8 %slice-start.2 = ((s8[16777216]{0:T(1024)(128)(4,1)}), s8[4194304]{0:T(1024)(128)(4,1)S(1)}, s32[]{:S(2)}) async-start(s8[16777216]{0:T(1024)(128)(4,1)} %bitcast.408), calls=%async_computation.5 | async-start | bytes 8388608
  157.7 7.9 %copy-start.9 = (bf16[512,512]{0,1:T(8,128)(2,1)S(1)}, bf16[512,512]{0,1:T(8,128)(2,1)}, u32[]{:S(2)}) copy-start(bf16[512,512]{0,1:T(8,128)(2,1)} %fusion.62) | copy-start | bytes 1572868
  157.7 10.1 %slice-start.3 = ((s8[16777216]{0:T(1024)(128)(4,1)}), s8[4194304]{0:T(1024)(128)(4,1)S(1)}, s32[]{:S(2)}) async-start(s8[16777216]{0:T(1024)(128)(4,1)} %bitcast.408), calls=%async_computation.6 | async-start | bytes 8388608
  159.1 6.5 %copy-start.6 = (f32[16,4,64,8,64]{2,4,1,0,3:T(8,128)}, f32[16,4,64,8,64]{2,4,1,0,3:T(8,128)S(1)}, u32[]{:S(2)}) copy-start(f32[16,4,64,8,64]{2,4,1,0,3:T(8,128)S(1)} %bitcast_dynamic-update-slice_fusion) | copy-start | bytes 25165828
  166.8 18.5 %copy-start.2 = (f32[4,512,1024]{1,2,0}, f32[4,512,1024]{1,2,0:S(1)}, u32[]{:S(2)}) copy-start(f32[4,512,1024]{1,2,0:S(1)} %fusion.123) | copy-start | bytes 25165828
  195.3 41.8 %collective-permute-start.1 = (bf16[4,64,1024]{2,1,0:T(8,128)(2,1)}, bf16[4,64,1024]{2,1,0:T(8,128)(2,1)}, u32[]{:S(2)}, u32[]{:S(2)}) collective-permute-start(bf16[4,64,1024]{2,1,0:T(8,128)(2,1)} %bitcast.25), channel_id=1, source_target_pairs={{4,0},{8,4},{12,8},{16,12},{20,16},{24,20},{28,24},{5,1},{9,5},{13... | collective-permute-start | bytes 1572872 | tf_op jit(solution)/shard_map/ppermute | solution.py:26
  198.7 40.0 %collective-permute-start = (bf16[4,64,1024]{2,1,0:T(8,128)(2,1)}, bf16[4,64,1024]{2,1,0:T(8,128)(2,1)}, u32[]{:S(2)}, u32[]{:S(2)}) collective-permute-start(bf16[4,64,1024]{2,1,0:T(8,128)(2,1)} %bitcast.24), channel_id=1, source_target_pairs={{0,4},{4,8},{8,12},{12,16},{16,20},{20,24},{24,28},{1,5},{5,9},{9,... | collective-permute-start | bytes 1572872 | tf_op jit(solution)/shard_map/ppermute | solution.py:24
  278.9 12.4 %copy-start.5 = (f32[4,512,512]{1,2,0:S(1)}, f32[4,512,512]{1,2,0}, u32[]{:S(2)}) copy-start(f32[4,512,512]{1,2,0} %copy-done.4) | copy-start | bytes 12582916
  292.6 6.8 %slice-start.6 = ((s8[8388608]{0:T(1024)(128)(4,1)}), s8[4194304]{0:T(1024)(128)(4,1)S(1)}, s32[]{:S(2)}) async-start(s8[8388608]{0:T(1024)(128)(4,1)} %bitcast.413), calls=%async_computation.9 | async-start | bytes 8388608
  292.6 8.4 %slice-start = ((s8[8388608]{0:T(1024)(128)(4,1)}), s8[4194304]{0:T(1024)(128)(4,1)S(1)}, s32[]{:S(2)}) async-start(s8[8388608]{0:T(1024)(128)(4,1)} %bitcast.403), calls=%async_computation.3 | async-start | bytes 8388608
  309.5 25.3 %all-to-all-start = ((bf16[4,384,512]{1,2,0:T(8,128)(2,1)}), bf16[4,384,512]{1,2,0:T(8,128)(2,1)}, u32[]{:S(2)}, u32[]{:S(2)}) async-start(bf16[4,384,512]{1,2,0:T(8,128)(2,1)} %copy.480), calls=%async_computation | async-start | bytes 3145728 | tf_op jit(solution)/shard_map/all_to_all | solution.py:203
  334.8 9.1 %copy-start.1 = (bf16[2048,512]{1,0:T(8,128)(2,1)S(1)}, bf16[2048,512]{1,0:T(8,128)(2,1)}, u32[]{:S(2)}) copy-start(bf16[2048,512]{1,0:T(8,128)(2,1)} %param.24) | copy-start | bytes 6291460
  (32 other events, 79.3 us)
Sparse Core Ops, SparseCore 0:
  9.5 52.0 all-gather.5
  63.1 44.8 all-gather.7
where the time goes:
time: 356 us; the launch traced here: 351 us
  local copies, waits for them, and re-layouts  104 us (29%)
  matrix products  89.7 us (25%)
  other arithmetic  75.7 us (21%)
  blocking collectives  55.5 us (16%)
  between operations  14.7 us (4%)
  starting transfers between devices  11 us (3%)
    dot_general x2, local copies, waits for them, and re-layouts, attend_rows(): jnp.einsum('nir,hrj,ckj->nhcik', row_onehot, offset_bias, col_onehot, pre...  27.8 us
    reduce_max x4, other arithmetic, attend_rows(): top = jnp.maximum(jnp.max(s_win, axis=(3, 4)), jnp.max(s_ctx, axis=3))  26.8 us
    dot_general x16, matrix products, attend_rows(): jnp.einsum('nchd,nkhd->nhck', queries, key_at(i), preferred_element_type=...  24.7 us
    psum x1, blocking collectives, shards(): summed = lax.psum((shift_part, scale_part, gate_part), 'sp')  24.2 us
    all_gather x1, blocking collectives, shards(): lax.all_gather(summed[2], 'tp', axis=0, tiled=True)  21 us
    dot_general x3, matrix products, attend_rows(): jnp.einsum('nir,hrj,ckj->nhcik', row_onehot, offset_bias, col_onehot, pre...  19.2 us
    unnamed x105, local copies, waits for them, and re-layouts  19 us
    reduce_sum x4, other arithmetic, attend_rows(): total = jnp.sum(e_win, axis=(3, 4)) + jnp.sum(e_ctx, axis=3)  17.2 us
  transfers between devices with their start and end apart: 5, of which 0 were waited for; matrix products, arithmetic and copies ran while one was open for 28% of the time, Pallas kernels for 0%

commit v1 on v0

v1 whole, which is shorter than its diff:
```python
import functools

import jax
import jax.numpy as jnp
from jax import lax
from jax.experimental import pallas as pl
from jax.experimental.pallas import tpu as pltpu
from jax.sharding import PartitionSpec as P

HEAD_DIM = 128
GRID_W = 64
WIN_ROWS = 8
WIN_COLS = 16
REACH = WIN_ROWS // 2
EPS = 1e-06
LOG2E = 1.4426950408889634
MASKED = -1e30
VMEM_BYTES = 60 * 1024 * 1024


def normed_tokens(rows, gain):
    floats = rows.astype(jnp.float32)
    inverse = lax.rsqrt(jnp.mean(floats * floats, axis=-1, keepdims=True) + EPS)
    return floats * inverse * gain


def store_heads(out_ref, at, values, gain):
    for h in range(values.shape[1] // HEAD_DIM):
        part = values[:, h * HEAD_DIM : (h + 1) * HEAD_DIM]
        part = part * lax.rsqrt(jnp.mean(part * part, axis=-1, keepdims=True) + EPS) * gain
        out_ref[:, at + h * HEAD_DIM : at + (h + 1) * HEAD_DIM] = part.astype(jnp.bfloat16)


def dot32(a, b):
    return jnp.dot(a, b, preferred_element_type=jnp.float32)


def dot_t(a, b):
    return lax.dot_general(a, b, (((1,), (1,)), ((), ())), preferred_element_type=jnp.float32)


def qkv_kernel(x_ref, scale_ref, shift_ref, gain_ref, wq, wk, wv, qg, kg, q_ref, kv_ref):
    normed = normed_tokens(x_ref[...], gain_ref[...]) * (1.0 + scale_ref[...]) + shift_ref[...]
    normed = normed.astype(jnp.bfloat16)
    width = wq.shape[1]
    store_heads(q_ref, 0, dot32(normed, wq[...]), qg[...])
    store_heads(kv_ref, 0, dot32(normed, wk[...]), kg[...])
    kv_ref[:, width:] = dot32(normed, wv[...]).astype(jnp.bfloat16)


def context_kernel(x_ref, gain_ref, wk, wv, kg, kv_ref):
    normed = normed_tokens(x_ref[...], gain_ref[...]).astype(jnp.bfloat16)
    width = wk.shape[1]
    store_heads(kv_ref, 0, dot32(normed, wk[...]), kg[...])
    kv_ref[:, width:] = dot32(normed, wv[...]).astype(jnp.bfloat16)


def fill_bias(ob_ref, table):
    lane = lax.broadcasted_iota(jnp.int32, (GRID_W, 2 * GRID_W), 1)
    query = lax.broadcasted_iota(jnp.int32, (GRID_W, 2 * GRID_W), 0)
    key = lane % GRID_W
    begin = jnp.clip(query - WIN_COLS // 2, 0, GRID_W - WIN_COLS)
    valid = (key >= begin) & (key < begin + WIN_COLS)
    lanes = 2 * GRID_W
    for r in range(2 * WIN_ROWS - 2):
        low = jnp.broadcast_to(ob_ref[0, r : r + 1, :], (GRID_W, lanes))
        high = jnp.broadcast_to(ob_ref[0, r + 1 : r + 2, :], (GRID_W, lanes))
        low = pltpu.roll(low, lanes - (WIN_COLS - 1), 1, stride=1, stride_axis=0)
        high = pltpu.roll(high, GRID_W - (WIN_COLS - 1), 1, stride=1, stride_axis=0)
        both = jnp.where(lane < GRID_W, low, high) * LOG2E
        table[r] = jnp.where(valid, both, MASKED)


def attention_kernel(
    block, total_rows, cb_ref, q_ref, k_ref, v_ref, kt, vt, kb, vb, ck_ref, cv_ref, ob_ref, out_ref,
    table, kbuf, vbuf
):
    fill_bias(ob_ref, table)
    rows = q_ref.shape[0] // GRID_W
    edge = REACH * GRID_W
    size = k_ref.shape[0]
    for buf, top, mid, low in ((kbuf, kt, k_ref, kb), (vbuf, vt, v_ref, vb)):
        buf[0:edge, :] = top[...]
        buf[edge : edge + size, :] = mid[...]
        buf[edge + size :, :] = low[...]
    first = lax.axis_index("sp") * rows
    context_bias = cb_ref[pl.program_id(0)] * LOG2E
    factor = HEAD_DIM ** (-0.5) * LOG2E
    span = WIN_ROWS * GRID_W

    def step(j, carry):
        base = pl.multiple_of(j * (block * GRID_W), block * GRID_W)
        queries = q_ref[pl.ds(base, block * GRID_W), :]
        s_ctx_all = dot_t(queries, ck_ref[...])
        p_ctx_all, outs = [], []
        for i in range(block):
            row = first + j * block + i
            start = jnp.clip(row - REACH, 0, total_rows - WIN_ROWS)
            r0 = start - row + WIN_ROWS - 1
            at = pl.multiple_of((start - first + REACH) * GRID_W, GRID_W)
            keys = kbuf[pl.ds(at, span), :]
            s_win = dot_t(queries[i * GRID_W : (i + 1) * GRID_W], keys) * factor
            bias = jnp.concatenate([table[r0 + 2 * m] for m in range(WIN_ROWS // 2)], axis=1)
            s_win = s_win + bias
            s_ctx = s_ctx_all[i * GRID_W : (i + 1) * GRID_W] * factor + context_bias
            top = jnp.maximum(
                jnp.max(s_win, axis=1, keepdims=True), jnp.max(s_ctx, axis=1, keepdims=True)
            )
            e_win = jnp.exp2(s_win - top)
            e_ctx = jnp.exp2(s_ctx - top)
            total = jnp.sum(e_win, axis=1, keepdims=True) + jnp.sum(e_ctx, axis=1, keepdims=True)
            inverse = 1.0 / total
            p_win = (e_win * inverse).astype(jnp.bfloat16)
            p_ctx_all.append((e_ctx * inverse).astype(jnp.bfloat16))
            outs.append(dot32(p_win, vbuf[pl.ds(at, span), :]))
        out = jnp.concatenate(outs, axis=0) + dot32(
            jnp.concatenate(p_ctx_all, axis=0), cv_ref[...]
        )
        out_ref[pl.ds(base, block * GRID_W), :] = out.astype(jnp.bfloat16)
        return carry

    lax.fori_loop(0, rows // block, step, 0)


def divisor(count, most):
    return max(d for d in range(1, most + 1) if count % d == 0)


def params(semantics):
    return pltpu.CompilerParams(dimension_semantics=semantics, vmem_limit_bytes=VMEM_BYTES)


def project(piece, scale, shift, gain, wq, wk, wv, qg, kg):
    tokens, d = piece.shape
    width = wq.shape[1]
    block = GRID_W * divisor(tokens // GRID_W, 4)
    whole = lambda a: pl.BlockSpec(a.shape, lambda i: (0, 0))
    args = (piece, scale, shift, gain, wq, wk, wv, qg, kg)
    return pl.pallas_call(
        qkv_kernel,
        grid=(tokens // block,),
        in_specs=[pl.BlockSpec((block, d), lambda i: (i, 0))] + [whole(a) for a in args[1:]],
        out_specs=[
            pl.BlockSpec((block, width), lambda i: (i, 0)),
            pl.BlockSpec((block, 2 * width), lambda i: (i, 0)),
        ],
        out_shape=[
            jax.ShapeDtypeStruct((tokens, width), jnp.bfloat16),
            jax.ShapeDtypeStruct((tokens, 2 * width), jnp.bfloat16),
        ],
        compiler_params=params(("arbitrary",)),
        cost_estimate=pl.CostEstimate(
            flops=6 * tokens * d * width,
            bytes_accessed=2 * (tokens * d + 3 * d * width + 3 * tokens * width),
            transcendentals=0,
        ),
        name="project",
    )(*args)


def project_context(context, gain, wk, wv, kg):
    count, d = context.shape
    width = wk.shape[1]
    return pl.pallas_call(
        context_kernel,
        out_shape=jax.ShapeDtypeStruct((count, 2 * width), jnp.bfloat16),
        compiler_params=pltpu.CompilerParams(vmem_limit_bytes=VMEM_BYTES),
        cost_estimate=pl.CostEstimate(
            flops=4 * count * d * width, bytes_accessed=4 * d * width, transcendentals=0
        ),
        name="project_context",
    )(context, gain, wk, wv, kg)


def attend(query, key_value, above, below, ctx, offset_bias, context_bias, total_rows):
    tokens, width = query.shape
    heads = width // HEAD_DIM
    rows = tokens // GRID_W
    edge = REACH * GRID_W
    count = ctx.shape[0]
    padded = jnp.pad(
        offset_bias, ((0, 0), (0, 0), (0, 2 * GRID_W - offset_bias.shape[2]))
    )
    col = lambda n: pl.BlockSpec((n, HEAD_DIM), lambda h: (0, h))
    col2 = lambda n: pl.BlockSpec((n, HEAD_DIM), lambda h: (0, heads + h))
    return pl.pallas_call(
        functools.partial(attention_kernel, divisor(rows, 4), total_rows),
        grid=(heads,),
        in_specs=[
            pl.BlockSpec(memory_space=pltpu.SMEM),
            col(tokens),
            col(tokens),
            col2(tokens),
            col(edge),
            col2(edge),
            col(edge),
            col2(edge),
            col(count),
            col2(count),
            pl.BlockSpec((1,) + padded.shape[1:], lambda h: (h, 0, 0)),
        ],
        out_specs=col(tokens),
        out_shape=jax.ShapeDtypeStruct((tokens, width), jnp.bfloat16),
        scratch_shapes=[
            pltpu.VMEM((2 * WIN_ROWS - 2, GRID_W, 2 * GRID_W), jnp.float32),
            pltpu.VMEM((tokens + 2 * edge, HEAD_DIM), jnp.bfloat16),
            pltpu.VMEM((tokens + 2 * edge, HEAD_DIM), jnp.bfloat16),
        ],
        compiler_params=params(("arbitrary",)),
        cost_estimate=pl.CostEstimate(
            flops=4 * tokens * width * (WIN_ROWS * GRID_W + count),
            bytes_accessed=8 * tokens * width,
            transcendentals=tokens * heads * (WIN_ROWS * GRID_W + count),
        ),
        name="attend",
    )(
        context_bias, query, key_value, key_value, above, above, below, below, ctx, ctx, padded
    )


def shards(
    resid,
    cond,
    mod_shift,
    mod_scale,
    mod_gate,
    norm_gain,
    context,
    w_query,
    w_key,
    w_value,
    query_gain,
    key_gain,
    offset_bias,
    context_bias,
    w_out,
):
    piece = lax.all_gather(resid, "tp", axis=0, tiled=True)
    gain = norm_gain[None, :]
    q_gain, k_gain = query_gain[None, :], key_gain[None, :]
    lifted = jax.nn.silu(cond.astype(jnp.float32)).astype(jnp.bfloat16)
    parts = jnp.stack(
        [
            jnp.dot(lifted, m, preferred_element_type=jnp.float32)
            for m in (mod_shift, mod_scale, mod_gate)
        ]
    )
    spread = lax.all_gather(parts, ("sp", "tp"), axis=0, tiled=False)
    sp, tp = lax.axis_size("sp"), lax.axis_size("tp")
    summed = jnp.sum(spread.reshape((sp, tp) + parts.shape), axis=0)
    shift, scale, gate = jnp.transpose(summed, (1, 0, 2)).reshape(3, 1, -1)
    ctx = project_context(context, gain, w_key, w_value, k_gain)
    ctx = lax.all_gather(ctx, "sp", axis=0, tiled=True)
    query, key_value = project(
        piece, scale, shift, gain, w_query, w_key, w_value, q_gain, k_gain
    )
    edge = REACH * GRID_W
    above = lax.ppermute(key_value[-edge:], "sp", [(i, i + 1) for i in range(sp - 1)])
    below = lax.ppermute(key_value[:edge], "sp", [(i + 1, i) for i in range(sp - 1)])
    total_rows = query.shape[0] // GRID_W * sp
    attended = attend(
        query, key_value, above, below, ctx, offset_bias, context_bias, total_rows
    )
    full_rows = lax.all_to_all(attended, "tp", split_axis=0, concat_axis=1, tiled=True)
    result = jnp.dot(full_rows, w_out, preferred_element_type=jnp.float32)
    return (resid.astype(jnp.float32) + gate * result).astype(jnp.bfloat16)


def solution(mesh):
    in_specs = (
        P(("sp", "tp"), None),
        P("sp"),
        P("sp", "tp"),
        P("sp", "tp"),
        P("sp", "tp"),
        P(),
        P("sp", None),
        P(None, "tp"),
        P(None, "tp"),
        P(None, "tp"),
        P(),
        P(),
        P("tp", None, None),
        P("tp"),
        P(),
    )
    out_specs = P(("sp", "tp"), None)
    return jax.shard_map(shards, mesh=mesh, in_specs=in_specs, out_specs=out_specs, check_vma=False)
```

time: 356 us -> 198 us (0.56)
  the two profiles are of different devices: /device:TPU:0 before, /device:TPU:4 now
where the time goes in v1:
time: 198 us; the launch traced here: 197 us
  Pallas kernels  63.9 us (32%)
  blocking collectives  62.6 us (32%)
  waiting for transfers between devices  37.4 us (19%)
  between operations  13.5 us (7%)
  matrix products  8.55 us (4%)
  starting transfers between devices  5.91 us (3%)
  local copies, waits for them, and re-layouts  5.42 us (3%)
    pallas_call x1, Pallas kernels, attend(): pl.pallas_call(functools.partial(attention_kernel, divisor(rows, 4), tota...  43.6 us
    all_gather x1, blocking collectives, shards(): spread = lax.all_gather(parts, ('sp', 'tp'), axis=0, tiled=False)  39.9 us
    all_gather x1, waiting for transfers between devices, shards(): ctx = lax.all_gather(ctx, 'sp', axis=0, tiled=True)  30.5 us
    all_to_all x1, blocking collectives, shards(): lax.all_to_all(attended, 'tp', split_axis=0, concat_axis=1, tiled=True)  22.6 us
    pallas_call x1, Pallas kernels, project(): pl.pallas_call(qkv_kernel, grid=(tokens // block,), in_specs=[pl.BlockSpe...  16.4 us
    dot_general x1, matrix products, shards(): result = jnp.dot(full_rows, w_out, preferred_element_type=jnp.float32)  8.12 us
    all_gather x1, waiting for transfers between devices, shards(): piece = lax.all_gather(resid, 'tp', axis=0, tiled=True)  6.13 us
    pallas_call x1, Pallas kernels, project_context(): pl.pallas_call(context_kernel, out_shape=jax.ShapeDtypeStruct((count, 2 *...  3.97 us
  transfers between devices with their start and end apart: 4, of which 2 were waited for; matrix products, arithmetic and copies ran while one was open for 2% of the time, Pallas kernels for 10%

profile of v1, /device:TPU:4, one launch (start us, length us, event | category | flops | bytes accessed | tf_op | source)
XLA Modules:
  0.0 197.4 jit_solution(14855816404837206279)
XLA Ops:
  6.5 0.7 all-gather.5.cloned.1.call-update
  7.3 0.0 all-gather.7.cloned.1.call-start
  7.3 4.0 %project_context.1 = bf16[64,1024]{1,0:T(8,128)(2,1)} custom-call(bf16[64,2048]{1,0:T(8,128)(2,1)} %x_ref.1, f32[1,2048]{1,0:T(1,128)} %bitcast.29, bf16[2048,512]{1,0:T(8,128)(2,1)} %wk.3, bf16[2048,512]{1,0:T(8,128)(2,1)} %wv.3, f32[1,128]{1,0:T(1,128)} %bitcast.34), custom_call_target="tpu_custom_call" | custom-call | flops 268435456 | bytes 4194304 | tf_op jit(solution)/shard_map/project_context/pallas_call | solution.py:164
  11.3 0.0 all-gather.7.cloned.1.call-update
  11.4 0.1 fusion.5
  11.5 0.1 fusion.6
  11.7 0.1 fusion.7
  11.8 39.9 %all-gather.1 = f32[32,3,512]{2,1,0:T(4,128)S(1)} all-gather(f32[1,3,512]{2,1,0:T(4,128)S(1)} %maximum_bitcast_fusion), channel_id=2, replica_groups=mesh['sp'=8,'tp'=4] {'sp','tp'}, dimensions={0}, use_global_device_ids=true | all-gather | bytes 202752 | tf_op jit(solution)/shard_map/all_gather | solution.py:248
  51.8 0.6 fusion.4
  52.5 6.1 %all-gather.5.cloned.1.call-done.x_ref = bf16[1536,2048]{1,0:T(8,128)(2,1)} async-done(((bf16[384,2048]{1,0:T(8,128)(2,1)}), bf16[1536,2048]{1,0:T(8,128)(2,1)}) %all-gather.5.cloned.1.call-update) | async-done | bytes 6291472 | tf_op jit(solution)/shard_map/all_gather | solution.py:238
  58.6 16.4 %project.1 = (bf16[1536,512]{1,0:T(8,128)(2,1)}, bf16[1536,1024]{1,0:T(8,128)(2,1)}) custom-call(bf16[1536,2048]{1,0:T(8,128)(2,1)} %all-gather.5.cloned.1.call-done.x_ref, f32[1,2048]{1,0:T(1,128)} %bitcast.33, f32[1,2048]{1,0:T(1,128)} %bitcast.32, f32[1,2048]{1,0:T(1,128)} %bitcast.30, bf16[2048,512]{1,0:T(8,128)(2,1)} %wq.1, bf16[2048,512]{1,0:T(8,128)(2,1)} %wk.3, ...), custom_call_target="tpu_custom_call" | custom-call | flops 9663676416 | bytes 17301504 | tf_op jit(solution)/shard_map/project/pallas_call | solution.py:139
  75.0 1.3 fusion.3
  76.2 3.1 %collective-permute-start = (bf16[256,1024]{1,0:T(8,128)(2,1)S(1)}, bf16[256,1024]{1,0:T(8,128)(2,1)S(1)}, u32[]{:S(2)}, u32[]{:S(2)}) collective-permute-start(bf16[256,1024]{1,0:T(8,128)(2,1)S(1)} %get-tuple-element.10), channel_id=1, source_target_pairs={{0,4},{4,8},{8,12},{12,16},{16,20},{20,24},{24,28},{1,5},{5,9},{9,... | collective-permute-start | bytes 1572872 | tf_op jit(solution)/shard_map/ppermute | solution.py:258
  79.3 2.8 %collective-permute-start.1 = (bf16[256,1024]{1,0:T(8,128)(2,1)S(1)}, bf16[256,1024]{1,0:T(8,128)(2,1)S(1)}, u32[]{:S(2)}, u32[]{:S(2)}) collective-permute-start(bf16[256,1024]{1,0:T(8,128)(2,1)S(1)} %get-tuple-element.9), channel_id=1, source_target_pairs={{4,0},{8,4},{12,8},{16,12},{20,16},{24,20},{28,24},{5,1},{9,5},{13... | collective-permute-start | bytes 1572872 | tf_op jit(solution)/shard_map/ppermute | solution.py:259
  82.1 0.6 pad.4.ob_ref
  82.8 30.5 %all-gather.7.cloned.1.call-done.ck_ref.cv_ref = bf16[512,1024]{1,0:T(8,128)(2,1)} async-done(((bf16[64,1024]{1,0:T(8,128)(2,1)}), bf16[512,1024]{1,0:T(8,128)(2,1)}) %all-gather.7.cloned.1.call-update) | async-done | bytes 1048592 | tf_op jit(solution)/shard_map/all_gather | solution.py:253
  113.3 0.0 collective-permute-done.kt.vt
  113.3 0.8 copy-done.1
  114.1 0.2 copy-done.2
  114.3 43.6 %attend.1 = bf16[1536,512]{1,0:T(8,128)(2,1)} custom-call(f32[4]{0:T(128)} %cb_ref.1, bf16[1536,512]{1,0:T(8,128)(2,1)} %get-tuple-element.7.q_ref, bf16[1536,1024]{1,0:T(8,128)(2,1)} %get-tuple-element.8.k_ref.v_ref, bf16[1536,1024]{1,0:T(8,128)(2,1)} %get-tuple-element.8.k_ref.v_ref, bf16[256,1024]{1,0:T(8,128)(2,1)} %copy-done.1, ...), custom_call_target="tpu_custom_call" | custom-call | flops 3221225472 | bytes 6291456 | tf_op jit(solution)/shard_map/attend/pallas_call | solution.py:186
  157.9 1.9 copy.22
  159.8 0.0 copy-start.3
  159.8 22.6 %all_to_all.19 = bf16[4,384,512]{1,2,0:T(8,128)(2,1)S(1)} all-to-all(bf16[4,384,512]{1,2,0:T(8,128)(2,1)S(1)} %copy.22), channel_id=1, replica_groups=mesh['sp'=8,'tp'=4] {'tp'}, dimensions={0} | all-to-all | bytes 3145728 | tf_op jit(solution)/shard_map/all_to_all | solution.py:264
  182.4 8.1 %add_convert_fusion = bf16[384,2048]{1,0:T(8,128)(2,1)} fusion(bf16[384,2048]{1,0:T(8,128)(2,1)S(1)} %copy-done.3, bf16[384,2048]{0,1:T(8,128)(2,1)S(1)} %bitcast.26, bf16[2048,2048]{1,0:T(8,128)(2,1)} %param.29, f32[2048]{0:T(1024)S(1)} %bitcast.31), kind=kOutput, calls=%fused_computation | convolution fusion | flops 3224371200 | bytes 13115392 | tf_op jit(solution)/shard_map/dot_general | solution.py:265
  (20 shorter events, 0.1 us)
Async XLA Ops:
  6.5 4.8 %copy-start = (bf16[256,512]{1,0:T(8,128)(2,1)S(1)}, bf16[256,512]{1,0:T(8,128)(2,1)}, u32[]{:S(2)}) copy-start(bf16[256,512]{1,0:T(8,128)(2,1)} %param.17) | copy-start | bytes 786436
  6.5 52.1 %all-gather.5.cloned.1.call-start = ((), (), s32[]{:S(2)}) async-start(), calls=%async_computation.1 | async-start | bytes 7864320 | tf_op jit(solution)/shard_map/all_gather | solution.py:238
  7.3 106.0 %all-gather.7.cloned.1.call-start = ((), (), s32[]{:S(2)}) async-start(), calls=%async_computation.2 | async-start | bytes 1179648 | tf_op jit(solution)/shard_map/all_gather | solution.py:253
  7.3 4.0 %copy-start.7 = (bf16[256]{0:T(256)(128)(2,1)S(1)}, bf16[256]{0:T(256)(128)(2,1)}, u32[]{:S(2)}) copy-start(bf16[256]{0:T(256)(128)(2,1)} %param.16) | copy-start | bytes 1540
  7.3 4.2 %copy-start.4 = (bf16[256,512]{1,0:T(8,128)(2,1)S(1)}, bf16[256,512]{1,0:T(8,128)(2,1)}, u32[]{:S(2)}) copy-start(bf16[256,512]{1,0:T(8,128)(2,1)} %param.18) | copy-start | bytes 786436
  7.3 4.3 %copy-start.5 = (bf16[256,512]{1,0:T(8,128)(2,1)S(1)}, bf16[256,512]{1,0:T(8,128)(2,1)}, u32[]{:S(2)}) copy-start(bf16[256,512]{1,0:T(8,128)(2,1)} %param.19) | copy-start | bytes 786436
  75.0 7.2 %copy-start.6 = (f32[4,15,31]{2,0,1:T(4,128)S(1)}, f32[4,15,31]{2,0,1:T(4,128)}, u32[]{:S(2)}) copy-start(f32[4,15,31]{2,0,1:T(4,128)} %param.27) | copy-start | bytes 22324
  76.2 37.0 %collective-permute-start = (bf16[256,1024]{1,0:T(8,128)(2,1)S(1)}, bf16[256,1024]{1,0:T(8,128)(2,1)S(1)}, u32[]{:S(2)}, u32[]{:S(2)}) collective-permute-start(bf16[256,1024]{1,0:T(8,128)(2,1)S(1)} %get-tuple-element.10), channel_id=1, source_target_pairs={{0,4},{4,8},{8,12},{12,16},{16,20},{20,24},{24,28},{1,5},{5,9},{9,... | collective-permute-start | bytes 1572872 | tf_op jit(solution)/shard_map/ppermute | solution.py:258
  79.3 34.0 %collective-permute-start.1 = (bf16[256,1024]{1,0:T(8,128)(2,1)S(1)}, bf16[256,1024]{1,0:T(8,128)(2,1)S(1)}, u32[]{:S(2)}, u32[]{:S(2)}) collective-permute-start(bf16[256,1024]{1,0:T(8,128)(2,1)S(1)} %get-tuple-element.9), channel_id=1, source_target_pairs={{4,0},{8,4},{12,8},{16,12},{20,16},{24,20},{28,24},{5,1},{9,5},{13... | collective-permute-start | bytes 1572872 | tf_op jit(solution)/shard_map/ppermute | solution.py:259
  113.3 0.8 copy-start.1
  113.3 1.0 copy-start.2
  159.8 22.6 %copy-start.3 = (bf16[384,2048]{1,0:T(8,128)(2,1)S(1)}, bf16[384,2048]{1,0:T(8,128)(2,1)}, u32[]{:S(2)}) copy-start(bf16[384,2048]{1,0:T(8,128)(2,1)} %param.15) | copy-start | bytes 4718596
Sparse Core Ops, SparseCore 0:
  8.9 49.6 all-gather.4
  60.7 52.5 all-gather.6

commit v2 on v1

v2 whole, which is shorter than its diff:
```python
import functools

import jax
import jax.numpy as jnp
from jax import lax
from jax.experimental import pallas as pl
from jax.experimental.pallas import tpu as pltpu
from jax.sharding import PartitionSpec as P

HEAD_DIM = 128
GRID_W = 64
WIN_ROWS = 8
WIN_COLS = 16
REACH = WIN_ROWS // 2
EPS = 1e-06
LOG2E = 1.4426950408889634
MASKED = -1e30
VMEM_BYTES = 60 * 1024 * 1024


def dot32(a, b):
    return jnp.dot(a, b, preferred_element_type=jnp.float32)


def dot_t(a, b):
    return lax.dot_general(a, b, (((1,), (1,)), ((), ())), preferred_element_type=jnp.float32)


def divisor(count, most):
    return max(d for d in range(1, most + 1) if count % d == 0)


def normed_tokens(rows, gain):
    floats = rows.astype(jnp.float32)
    inverse = lax.rsqrt(jnp.mean(floats * floats, axis=-1, keepdims=True) + EPS)
    return floats * inverse * gain


def store_heads(out_ref, at, values, gain):
    count = values.shape[0]
    for h in range(values.shape[1] // HEAD_DIM):
        part = values[:, h * HEAD_DIM : (h + 1) * HEAD_DIM]
        part = part * lax.rsqrt(jnp.mean(part * part, axis=-1, keepdims=True) + EPS) * gain
        out_ref[pl.ds(at, count), h * HEAD_DIM : (h + 1) * HEAD_DIM] = part.astype(jnp.bfloat16)


def fill_bias(ob_ref, table, h):
    lane = lax.broadcasted_iota(jnp.int32, (GRID_W, 2 * GRID_W), 1)
    query = lax.broadcasted_iota(jnp.int32, (GRID_W, 2 * GRID_W), 0)
    key = lane % GRID_W
    begin = jnp.clip(query - WIN_COLS // 2, 0, GRID_W - WIN_COLS)
    valid = (key >= begin) & (key < begin + WIN_COLS)
    lanes = 2 * GRID_W
    for r in range(2 * WIN_ROWS - 2):
        low = jnp.broadcast_to(ob_ref[h, r : r + 1, :], (GRID_W, lanes))
        high = jnp.broadcast_to(ob_ref[h, r + 1 : r + 2, :], (GRID_W, lanes))
        low = pltpu.roll(low, lanes - (WIN_COLS - 1), 1, stride=1, stride_axis=0)
        high = pltpu.roll(high, GRID_W - (WIN_COLS - 1), 1, stride=1, stride_axis=0)
        both = jnp.where(lane < GRID_W, low, high) * LOG2E
        table[h, r] = jnp.where(valid, both, MASKED)


def layer_kernel(
    sp, tp, chunks, cb_ref, resid, cond, mshift, mscale, mgate, gain_ref, context, wq_hbm, wk_hbm,
    wv_hbm, qg, kg, ob_ref, wo_hbm, out_ref,
    tok, wq, wk, wv, wo, qbuf, kvbuf, ctxbuf, table, modsp, modtp, mods, att, full,
    load_sem, tok_send, pair_send, fwd_send, tok_recv, msp_send, msp_recv, mtp_send, mtp_recv,
    ctx_send, ctx_recv, halo_send, halo_recv, att_send, att_recv,
):
    me_s, me_t = lax.axis_index("sp"), lax.axis_index("tp")
    count, d = resid.shape
    chunk = count // chunks
    width = wq.shape[1]
    heads = width // HEAD_DIM
    tokens = count * tp
    rows = tokens // GRID_W
    total_rows = rows * sp
    first = me_s * rows
    chips = tp // 2
    chip, core = me_t // 2, me_t % 2
    pair = chip * 2 + (1 - core)

    def remote(src, dst, send, recv, axis, peer):
        return pltpu.make_async_remote_copy(
            src_ref=src, dst_ref=dst, send_sem=send, recv_sem=recv,
            device_id={axis: peer}, device_id_type=pl.DeviceIdType.MESH,
        )

    loads = [
        pltpu.make_async_copy(a, b, load_sem.at[i])
        for i, (a, b) in enumerate(
            ((wk_hbm, wk), (wv_hbm, wv), (wq_hbm, wq), (wo_hbm, wo), (resid, tok.at[me_t]))
        )
    ]
    for copy in (loads[4], loads[0], loads[1], loads[2]):
        copy.start()

    barrier = pltpu.get_barrier_semaphore()
    for k in range(1, sp):
        pl.semaphore_signal(
            barrier, inc=1, device_id={"sp": lax.rem(me_s + k, sp)},
            device_id_type=pl.DeviceIdType.MESH,
        )
    for k in range(1, tp):
        pl.semaphore_signal(
            barrier, inc=1, device_id={"tp": lax.rem(me_t + k, tp)},
            device_id_type=pl.DeviceIdType.MESH,
        )
    pl.semaphore_wait(barrier, sp + tp - 2)

    def part(block, c):
        return tok.at[block, pl.ds(pl.multiple_of(c * chunk, chunk), chunk), :]

    def mine(c):
        return resid.at[pl.ds(pl.multiple_of(c * chunk, chunk), chunk), :]

    def across(k, c):
        peer = lax.rem(chip + k, chips) * 2 + core
        return remote(
            mine(c), part(me_t, c), tok_send.at[(k - 1) * chunks + c],
            tok_recv.at[me_t * chunks + c], "tp", peer,
        )

    def beside(c):
        return remote(
            mine(c), part(me_t, c), pair_send.at[c], tok_recv.at[me_t * chunks + c], "tp", pair
        )

    def onward(k, c):
        block = lax.rem(chip + k, chips) * 2 + core
        return remote(
            part(block, c), part(block, c), fwd_send.at[(k - 1) * chunks + c],
            tok_recv.at[block * chunks + c], "tp", pair,
        )

    def arrived(block, c):
        remote(
            part(block, c), part(block, c), pair_send.at[0], tok_recv.at[block * chunks + c],
            "tp", pair,
        ).wait_recv()

    for k in range(1, chips):
        across(k, 0).start()
    for c in range(chunks):
        beside(c).start()

    lifted = cond[...].astype(jnp.float32)
    lifted = (lifted / (1.0 + jnp.exp(-lifted))).astype(jnp.bfloat16)
    lifted = jnp.broadcast_to(lifted, (16, lifted.shape[1]))
    for i, m in enumerate((mshift, mscale, mgate)):
        modsp[me_s, i : i + 1, :] = dot32(lifted, m[...])[0:1]
    modsp[me_s, 3:8, :] = jnp.zeros((5, modsp.shape[2]), jnp.float32)

    def to_sp(k, buf, send, recv):
        return remote(
            buf.at[me_s], buf.at[me_s], send.at[k - 1], recv.at[me_s], "sp", lax.rem(me_s + k, sp)
        )

    def from_sp(k, buf, send, recv):
        peer = lax.rem(me_s + k, sp)
        remote(buf.at[peer], buf.at[peer], send.at[k - 1], recv.at[peer], "sp", peer).wait_recv()

    for k in range(1, sp):
        to_sp(k, modsp, msp_send, msp_recv).start()

    def fill(h, carry):
        fill_bias(ob_ref, table, h)
        return carry

    lax.fori_loop(0, heads, fill, 0)

    loads[0].wait()
    loads[1].wait()
    normed = normed_tokens(context[...], gain_ref[...]).astype(jnp.bfloat16)
    own = ctxbuf.at[me_s]
    store_heads(own, 0, dot32(normed, wk[...]), kg[...])
    own[:, width:] = dot32(normed, wv[...]).astype(jnp.bfloat16)

    for k in range(1, sp):
        from_sp(k, modsp, msp_send, msp_recv)
    summed = modsp[0]
    for s in range(1, sp):
        summed = summed + modsp[s]
    modtp[me_t] = summed

    def to_tp(k):
        return remote(
            modtp.at[me_t], modtp.at[me_t], mtp_send.at[k - 1], mtp_recv.at[me_t], "tp",
            lax.rem(me_t + k, tp),
        )

    for k in range(1, tp):
        to_tp(k).start()
    for k in range(1, sp):
        to_sp(k, ctxbuf, ctx_send, ctx_recv).start()
    for c in range(1, chunks):
        for k in range(1, chips):
            across(k, c).start()
    loads[3].start()
    loads[2].wait()
    loads[4].wait()
    for k in range(1, tp):
        peer = lax.rem(me_t + k, tp)
        remote(
            modtp.at[peer], modtp.at[peer], mtp_send.at[k - 1], mtp_recv.at[peer], "tp", peer
        ).wait_recv()
    piece = modtp.shape[2]
    for t in range(tp):
        mods[:, t * piece : (t + 1) * piece] = modtp[t]

    edge = REACH * GRID_W

    def project(block, c):
        values = tok[block, pl.ds(pl.multiple_of(c * chunk, chunk), chunk), :]
        normed = normed_tokens(values, gain_ref[...]) * (1.0 + mods[1:2, :]) + mods[0:1, :]
        normed = normed.astype(jnp.bfloat16)
        at = pl.multiple_of(block * count + c * chunk, chunk)
        store_heads(qbuf, at, dot32(normed, wq[...]), qg[...])
        at = pl.multiple_of(edge + block * count + c * chunk, GRID_W)
        store_heads(kvbuf, at, dot32(normed, wk[...]), kg[...])
        kvbuf[pl.ds(at, chunk), width:] = dot32(normed, wv[...]).astype(jnp.bfloat16)

    def local_step(c, carry):
        project(me_t, c)
        return carry

    lax.fori_loop(0, chunks, local_step, 0)

    def pair_step(c, carry):
        arrived(pair, c)
        project(pair, c)
        return carry

    lax.fori_loop(0, chunks, pair_step, 0)

    def far_step(i, carry):
        c = i % chunks
        k = 1 + i // chunks
        near = lax.rem(chip + k, chips) * 2 + core
        other = lax.rem(chip + k, chips) * 2 + (1 - core)
        arrived(near, c)
        onward(k, c).start()
        project(near, c)
        arrived(other, c)
        project(other, c)
        return carry

    lax.fori_loop(0, (chips - 1) * chunks, far_step, 0)

    def up():
        return remote(
            kvbuf.at[pl.ds(edge, edge), :], kvbuf.at[pl.ds(edge + tokens, edge), :],
            halo_send.at[0], halo_recv.at[0], "sp", me_s - 1,
        )

    def down():
        return remote(
            kvbuf.at[pl.ds(tokens, edge), :], kvbuf.at[pl.ds(0, edge), :],
            halo_send.at[1], halo_recv.at[1], "sp", me_s + 1,
        )

    @pl.when(me_s > 0)
    def _():
        up().start()

    @pl.when(me_s < sp - 1)
    def _():
        down().start()

    for k in range(1, sp):
        from_sp(k, ctxbuf, ctx_send, ctx_recv)

    ctx_count = ctxbuf.shape[0] * ctxbuf.shape[1]
    factor = HEAD_DIM ** (-0.5) * LOG2E
    span = WIN_ROWS * GRID_W
    chunk_rows = rows // tp
    block = divisor(chunk_rows, 3)
    size = block * GRID_W

    def attend(dest, sub, h):
        lanes_k = pl.ds(pl.multiple_of(h * HEAD_DIM, HEAD_DIM), HEAD_DIM)
        lanes_v = pl.ds(pl.multiple_of(width + h * HEAD_DIM, HEAD_DIM), HEAD_DIM)
        row0 = dest * chunk_rows + sub * block
        queries = qbuf[pl.ds(pl.multiple_of(row0 * GRID_W, GRID_W), size), lanes_k]
        ctx_key = ctxbuf[:, :, lanes_k].reshape(ctx_count, HEAD_DIM)
        ctx_value = ctxbuf[:, :, lanes_v].reshape(ctx_count, HEAD_DIM)
        context_bias = cb_ref[h] * LOG2E
        s_ctx_all = dot_t(queries, ctx_key)
        p_ctx_all, outs = [], []
        for i in range(block):
            row = first + row0 + i
            start = jnp.clip(row - REACH, 0, total_rows - WIN_ROWS)
            r0 = start - row + WIN_ROWS - 1
            at = pl.multiple_of((start - first + REACH) * GRID_W, GRID_W)
            s_win = dot_t(queries[i * GRID_W : (i + 1) * GRID_W], kvbuf[pl.ds(at, span), lanes_k])
            bias = jnp.concatenate([table[h, r0 + 2 * m] for m in range(WIN_ROWS // 2)], axis=1)
            s_win = s_win * factor + bias
            s_ctx = s_ctx_all[i * GRID_W : (i + 1) * GRID_W] * factor + context_bias
            top = jnp.maximum(
                jnp.max(s_win, axis=1, keepdims=True), jnp.max(s_ctx, axis=1, keepdims=True)
            )
            e_win = jnp.exp2(s_win - top)
            e_ctx = jnp.exp2(s_ctx - top)
            total = jnp.sum(e_win, axis=1, keepdims=True) + jnp.sum(e_ctx, axis=1, keepdims=True)
            inverse = 1.0 / total
            p_ctx_all.append((e_ctx * inverse).astype(jnp.bfloat16))
            p_win = (e_win * inverse).astype(jnp.bfloat16)
            outs.append(dot32(p_win, kvbuf[pl.ds(at, span), lanes_v]))
        out = jnp.concatenate(outs, axis=0)
        out = out + dot32(jnp.concatenate(p_ctx_all, axis=0), ctx_value)
        att[dest, pl.ds(pl.multiple_of(sub * size, size), size), lanes_k] = out.astype(jnp.bfloat16)

    def hand(dest):
        return remote(
            att.at[dest], full.at[me_t], att_send.at[dest], att_recv.at[me_t], "tp", dest
        )

    def position(i, carry):
        step = i // 2
        forward = tp // 2 + step - (i % 2) * (2 * step + 1)
        low = jnp.where(chip < (chips + 1) // 2, 1, 0)
        dest = low * forward + (1 - low) * (tp - 1 - forward)

        def unit(j, inner):
            attend(dest, j // heads, j % heads)
            return inner

        lax.fori_loop(0, chunk_rows // block * heads, unit, 0)

        @pl.when(dest != me_t)
        def _():
            hand(dest).start()

        return carry

    free = max(0, 2 * (tp // 2 - -(-REACH // chunk_rows)))
    lax.fori_loop(0, free, position, 0)

    @pl.when(me_s > 0)
    def _():
        down().wait_recv()

    @pl.when(me_s < sp - 1)
    def _():
        up().wait_recv()

    lax.fori_loop(free, tp, position, 0)

    full[me_t] = att[me_t]
    loads[3].wait()
    for k in range(1, tp):
        peer = lax.rem(me_t + k, tp)
        remote(
            att.at[peer], full.at[peer], att_send.at[peer], att_recv.at[peer], "tp", peer
        ).wait_recv()

    tile = HEAD_DIM * divisor(d // HEAD_DIM, 4)

    def finish(j, carry):
        lanes = pl.ds(pl.multiple_of(j * tile, tile), tile)
        result = dot32(full[0], wo[0:width, lanes])
        for t in range(1, tp):
            result = result + dot32(full[t], wo[t * width : (t + 1) * width, lanes])
        floats = tok[me_t, :, lanes].astype(jnp.float32)
        out_ref[:, lanes] = (floats + mods[2:3, lanes] * result).astype(jnp.bfloat16)
        return carry

    lax.fori_loop(0, d // tile, finish, 0)

    for c in range(chunks):
        beside(c).wait_send()
        for k in range(1, chips):
            across(k, c).wait_send()
            onward(k, c).wait_send()
    for k in range(1, sp):
        to_sp(k, modsp, msp_send, msp_recv).wait_send()
        to_sp(k, ctxbuf, ctx_send, ctx_recv).wait_send()
    for k in range(1, tp):
        to_tp(k).wait_send()
        hand(lax.rem(me_t + k, tp)).wait_send()

    @pl.when(me_s > 0)
    def _():
        up().wait_send()

    @pl.when(me_s < sp - 1)
    def _():
        down().wait_send()


def shards(
    resid,
    cond,
    mod_shift,
    mod_scale,
    mod_gate,
    norm_gain,
    context,
    w_query,
    w_key,
    w_value,
    query_gain,
    key_gain,
    offset_bias,
    context_bias,
    w_out,
):
    sp, tp = lax.axis_size("sp"), lax.axis_size("tp")
    count, d = resid.shape
    width = w_query.shape[1]
    heads = width // HEAD_DIM
    tokens = count * tp
    padded = jnp.pad(offset_bias, ((0, 0), (0, 1), (0, 2 * GRID_W - offset_bias.shape[2])))
    chunks = divisor(count // GRID_W, 3)
    chips = tp // 2
    bf, f32 = jnp.bfloat16, jnp.float32
    piece = mod_shift.shape[1]
    vmem = pl.BlockSpec(memory_space=pltpu.VMEM)
    hbm = pl.BlockSpec(memory_space=pl.ANY)
    sems = pltpu.SemaphoreType.DMA
    hops = max(1, (chips - 1) * chunks)
    return pl.pallas_call(
        functools.partial(layer_kernel, sp, tp, chunks),
        in_specs=[pl.BlockSpec(memory_space=pltpu.SMEM), hbm]
        + [vmem] * 6
        + [hbm] * 3
        + [vmem] * 3
        + [hbm],
        out_specs=vmem,
        out_shape=jax.ShapeDtypeStruct((count, d), bf),
        scratch_shapes=[
            pltpu.VMEM((tp, count, d), bf),
            pltpu.VMEM((d, width), bf),
            pltpu.VMEM((d, width), bf),
            pltpu.VMEM((d, width), bf),
            pltpu.VMEM((width * tp, d), bf),
            pltpu.VMEM((tokens, width), bf),
            pltpu.VMEM((tokens + 2 * REACH * GRID_W, 2 * width), bf),
            pltpu.VMEM((sp, context.shape[0], 2 * width), bf),
            pltpu.VMEM((heads, 2 * WIN_ROWS - 2, GRID_W, 2 * GRID_W), f32),
            pltpu.VMEM((sp, 8, piece), f32),
            pltpu.VMEM((tp, 8, piece), f32),
            pltpu.VMEM((8, d), f32),
            pltpu.VMEM((tp, count, width), bf),
            pltpu.VMEM((tp, count, width), bf),
            sems((5,)),
            sems((hops,)),
            sems((chunks,)),
            sems((hops,)),
            sems((tp * chunks,)),
            sems((sp,)),
            sems((sp,)),
            sems((tp,)),
            sems((tp,)),
            sems((sp,)),
            sems((sp,)),
            sems((2,)),
            sems((2,)),
            sems((tp,)),
            sems((tp,)),
        ],
        compiler_params=pltpu.CompilerParams(
            collective_id=0, has_side_effects=True, vmem_limit_bytes=VMEM_BYTES
        ),
        name="layer",
    )(
        context_bias, resid, cond[None, :], mod_shift, mod_scale, mod_gate, norm_gain[None, :],
        context, w_query, w_key, w_value, query_gain[None, :], key_gain[None, :], padded, w_out,
    )


def solution(mesh):
    in_specs = (
        P(("sp", "tp"), None),
        P("sp"),
        P("sp", "tp"),
        P("sp", "tp"),
        P("sp", "tp"),
        P(),
        P("sp", None),
        P(None, "tp"),
        P(None, "tp"),
        P(None, "tp"),
        P(),
        P(),
        P("tp", None, None),
        P("tp"),
        P(),
    )
    out_specs = P(("sp", "tp"), None)
    return jax.shard_map(shards, mesh=mesh, in_specs=in_specs, out_specs=out_specs, check_vma=False)
```

time: 198 us -> 103 us (0.52)
  blocking collectives: 62.6 us -> 0 us
  waiting for transfers between devices: 37.4 us -> 0 us
  Pallas kernels: 63.9 us -> 97 us
  between operations: 13.5 us -> 0.01 us
  matrix products: 8.55 us -> 0 us
  starting transfers between devices: 5.91 us -> 0 us
    all_gather x1 -> x0, blocking collectives: 39.9 us -> none  [shards(): spread = lax.all_gather(parts, ('sp', 'tp'), axis=0, tiled=False)]
    all_gather x2 -> x0, waiting for transfers between devices: 36.6 us -> none  [the longest x1 30.5 us: shards(): ctx = lax.all_gather(ctx, 'sp', axis=0, tiled=True)]
    pallas_call x3 -> x1, Pallas kernels: 63.9 us -> 97 us  [shards(): pl.pallas_call(functools.partial(layer_kernel, sp, tp, chunks), in_specs=...]
    all_to_all x1 -> x0, blocking collectives: 22.6 us -> none  [shards(): lax.all_to_all(attended, 'tp', split_axis=0, concat_axis=1, tiled=True)]
    dot_general x4 -> x0, matrix products: 8.55 us -> none  [the longest x1 8.12 us: shards(): result = jnp.dot(full_rows, w_out, preferred_element_type=jnp.float32)]
    ppermute x2 -> x0, starting transfers between devices: 5.87 us -> none  [the longest x1 3.06 us: shards(): lax.ppermute(key_value[-edge:], 'sp', [(i, i + 1) for i in range(sp - 1)])]
    unnamed x17 -> x2, local copies, waits for them, and re-layouts: 1.03 us -> 3.48 us
  transfers between devices with their start and end apart: 4 -> 0, of which waited for: 2 -> 0; matrix products, arithmetic and copies ran while one was open for 2% -> 0% of each run, Pallas kernels for 10% -> 0%
where the time goes in v2:
time: 103 us; the launch traced here: 102 us
  Pallas kernels  97 us (94%)
  local copies, waits for them, and re-layouts  5.33 us (5%)
    pallas_call x1, Pallas kernels, shards(): pl.pallas_call(functools.partial(layer_kernel, sp, tp, chunks), in_specs=...  97 us
    unnamed x2, local copies, waits for them, and re-layouts  3.48 us

profile of v2, /device:TPU:4, one launch (start us, length us, event | category | flops | bytes accessed | tf_op | source)
XLA Modules:
  0.0 102.3 jit_solution(15142867388309236500)
XLA Ops:
  0.0 1.2 %broadcast_in_dim.12.cond = bf16[1,256]{1,0:T(2,128)(2,1)} reshape(bf16[256]{0:T(256)(128)(2,1)} %param.16) | data formatting | bytes 1024 | tf_op jit(solution)/shard_map/broadcast_in_dim | solution.py:467
  1.2 0.8 copy.16
  2.0 0.6 pad.4.ob_ref
  2.6 97.0 %layer.1 = bf16[384,2048]{1,0:T(8,128)(2,1)} custom-call(f32[4]{0:T(128)} %cb_ref.1, bf16[384,2048]{1,0:T(8,128)(2,1)} %resid.1, bf16[1,256]{1,0:T(2,128)(2,1)} %broadcast_in_dim.12.cond, bf16[256,512]{1,0:T(8,128)(2,1)} %mshift.1, bf16[256,512]{1,0:T(8,128)(2,1)} %mscale.1, bf16[256,512]{1,0:T(8,128)(2,1)} %mgate.1, f32[1,2048]{1,0:T(1,128)} %bitcast.3, ...), custom_call_target="tpu_custom_call" | custom-call | tf_op jit(solution)/shard_map/layer/pallas_call | solution.py:422
  99.6 2.7 %copy.18 = bf16[384,2048]{1,0:T(8,128)(2,1)} copy(bf16[384,2048]{1,0:T(8,128)(2,1)} %layer.1) | data formatting | bytes 3145728

commit v3 on v2

--- a/solution.py
+++ b/solution.py
@@ -163,12 +163,6 @@
     for k in range(1, sp):
         to_sp(k, modsp, msp_send, msp_recv).start()
 
-    def fill(h, carry):
-        fill_bias(ob_ref, table, h)
-        return carry
-
-    lax.fori_loop(0, heads, fill, 0)
-
     loads[0].wait()
     loads[1].wait()
     normed = normed_tokens(context[...], gain_ref[...]).astype(jnp.bfloat16)
@@ -196,6 +190,12 @@
     for c in range(1, chunks):
         for k in range(1, chips):
             across(k, c).start()
+    def fill(h, carry):
+        fill_bias(ob_ref, table, h)
+        return carry
+
+    lax.fori_loop(0, heads, fill, 0)
+
     loads[3].start()
     loads[2].wait()
     loads[4].wait()
@@ -286,7 +286,7 @@
         ctx_value = ctxbuf[:, :, lanes_v].reshape(ctx_count, HEAD_DIM)
         context_bias = cb_ref[h] * LOG2E
         s_ctx_all = dot_t(queries, ctx_key)
-        p_ctx_all, outs = [], []
+        p_ctx_all, outs, inverses = [], [], []
         for i in range(block):
             row = first + row0 + i
             start = jnp.clip(row - REACH, 0, total_rows - WIN_ROWS)
@@ -302,12 +302,13 @@
             e_win = jnp.exp2(s_win - top)
             e_ctx = jnp.exp2(s_ctx - top)
             total = jnp.sum(e_win, axis=1, keepdims=True) + jnp.sum(e_ctx, axis=1, keepdims=True)
-            inverse = 1.0 / total
-            p_ctx_all.append((e_ctx * inverse).astype(jnp.bfloat16))
-            p_win = (e_win * inverse).astype(jnp.bfloat16)
+            inverses.append(1.0 / total)
+            p_ctx_all.append(e_ctx.astype(jnp.bfloat16))
+            p_win = e_win.astype(jnp.bfloat16)
             outs.append(dot32(p_win, kvbuf[pl.ds(at, span), lanes_v]))
         out = jnp.concatenate(outs, axis=0)
         out = out + dot32(jnp.concatenate(p_ctx_all, axis=0), ctx_value)
+        out = out * jnp.concatenate(inverses, axis=0)
         att[dest, pl.ds(pl.multiple_of(sub * size, size), size), lanes_k] = out.astype(jnp.bfloat16)
 
     def hand(dest):

time: 103 us -> 99.1 us (0.962)
  Pallas kernels: 97 us -> 93.6 us
    pallas_call x1, Pallas kernels: 97 us -> 93.6 us  [shards(): pl.pallas_call(functools.partial(layer_kernel, sp, tp, chunks), in_specs=...]
where the time goes in v3:
time: 99.1 us; the launch traced here: 98.9 us
  Pallas kernels  93.6 us (94%)
  local copies, waits for them, and re-layouts  5.33 us (5%)
    pallas_call x1, Pallas kernels, shards(): pl.pallas_call(functools.partial(layer_kernel, sp, tp, chunks), in_specs=...  93.6 us
    unnamed x2, local copies, waits for them, and re-layouts  3.48 us

profile of v3, /device:TPU:4, one launch (start us, length us, event | category | flops | bytes accessed | tf_op | source)
XLA Modules:
  0.0 98.9 jit_solution(7796968069171103795)
XLA Ops:
  0.0 1.2 %broadcast_in_dim.12.cond = bf16[1,256]{1,0:T(2,128)(2,1)} reshape(bf16[256]{0:T(256)(128)(2,1)} %param.16) | data formatting | bytes 1024 | tf_op jit(solution)/shard_map/broadcast_in_dim | solution.py:468
  1.2 0.8 copy.16
  2.0 0.6 pad.4.ob_ref
  2.6 93.6 %layer.1 = bf16[384,2048]{1,0:T(8,128)(2,1)} custom-call(f32[4]{0:T(128)} %cb_ref.1, bf16[384,2048]{1,0:T(8,128)(2,1)} %resid.1, bf16[1,256]{1,0:T(2,128)(2,1)} %broadcast_in_dim.12.cond, bf16[256,512]{1,0:T(8,128)(2,1)} %mshift.1, bf16[256,512]{1,0:T(8,128)(2,1)} %mscale.1, bf16[256,512]{1,0:T(8,128)(2,1)} %mgate.1, f32[1,2048]{1,0:T(1,128)} %bitcast.3, ...), custom_call_target="tpu_custom_call" | custom-call | tf_op jit(solution)/shard_map/layer/pallas_call | solution.py:423
  96.2 2.7 %copy.18 = bf16[384,2048]{1,0:T(8,128)(2,1)} copy(bf16[384,2048]{1,0:T(8,128)(2,1)} %layer.1) | data formatting | bytes 3145728
